TPU v7x, 32 devices: a whole 2x2x4 slice. The times are simulated.
32 devices in a mesh: sp: 16 (over z, x, core), tp: 2 (over y).
Axes of the slice: x: 2, y: 2, z: 4, core: 2. Of those that a mesh axis runs over, the one named last changes fastest.
Arguments:
- stream: bfloat16 [4096, 2048], P('sp'), may hold values from -6 to 6
- doc_ids: int32 [4096], P('sp'), may hold values from 0 to 3, never falling along the last dimension, each value on 1 to 2048 neighbouring positions
- norm_gain: float32 [2, 2048], replicated, may hold values from 0.1 to 1.9
- w_query: bfloat16 [2, 2048, 1024], P(None, None, 'tp'), may hold values from -0.125 to 0.125
- w_key: bfloat16 [2, 2048, 1024], P(None, None, 'tp'), may hold values from -0.125 to 0.125
- w_value: bfloat16 [2, 2048, 1024], P(None, None, 'tp'), may hold values from -0.125 to 0.125
- query_gain: float32 [2, 64], replicated, may hold values from 0.4 to 7
- key_gain: float32 [2, 64], replicated, may hold values from 0.4 to 7
- offset_bias: float32 [2, 16, 8, 16], P(None, 'tp'), may hold values from -4 to 4
- w_output: bfloat16 [2, 1024, 2048], replicated, may hold values from -0.1875 to 0.1875
Outputs:
- result: bfloat16 [4096, 2048], P('sp')
Inputs may be any that keep to these rules, and one draw needn't show every extreme that they name: `doc_ids`: numbers never fall along the sequence; each document holds 1 to 2048 positions and one holds exactly 2048.
All inputs are finite; a program needn't handle non-finite values.
Results may differ from a plain program's by a relative error of at most 0.034.
The roundings to bfloat16 on the way count: a program that leaves them out, or rounds other values in their place, can miss the bound.
Values may be sent and summed in bfloat16 or wider, within the bound.
No kernel may reach another device: no remote copies, remote signals or barrier semaphores. Data moves between devices by JAX's collectives and lax.ppermute only.
A program may use at most 128 MiB of HBM per device.

v0:
```python
import jax
import jax.numpy as jnp
from jax import lax
from jax.sharding import PartitionSpec as P

HEAD_DIM = 64
GRID_W = 64
WIN_ROWS = 8
WIN_COLS = 16


eps = 1e-06


def padded(block, sides, width):
    for axis, dim in sides:
        count = lax.axis_size(axis)
        forward = [(i, i + 1) for i in range(count - 1)]
        backward = [(target, source) for source, target in forward]
        low = lax.ppermute(
            lax.slice_in_dim(block, block.shape[dim] - width, None, axis=dim), axis, forward
        )
        high = lax.ppermute(lax.slice_in_dim(block, 0, width, axis=dim), axis, backward)
        block = jnp.concatenate([low, block, high], axis=dim)
    return block


def head_norm(raw_rows, gain_row):
    split_rows = raw_rows.reshape(raw_rows.shape[0], -1, HEAD_DIM)
    inverse = lax.rsqrt(jnp.mean(split_rows * split_rows, axis=-1, keepdims=True) + eps)
    return (split_rows * inverse * gain_row).astype(jnp.bfloat16).reshape(raw_rows.shape)


def project(layer_params, row_block):
    gain_vector, query_weight, key_weight, value_weight, query_scale, key_scale = layer_params
    token_rows = row_block.astype(jnp.float32)
    inv_rms = lax.rsqrt(jnp.mean(token_rows * token_rows, axis=-1, keepdims=True) + eps)
    normed = (token_rows * inv_rms * gain_vector).astype(jnp.bfloat16)
    queries = head_norm(
        jnp.dot(normed, query_weight, preferred_element_type=jnp.float32), query_scale
    )
    key_rows = head_norm(jnp.dot(normed, key_weight, preferred_element_type=jnp.float32), key_scale)
    value_rows = jnp.dot(normed, value_weight, preferred_element_type=jnp.float32).astype(
        jnp.bfloat16
    )
    return jnp.concatenate([queries, key_rows, value_rows], axis=1)


def offset_table(head_bias):
    key_reach = 2 * WIN_COLS - 1
    offsets = (
        jnp.arange(key_reach, dtype=jnp.int32)[None, :]
        - jnp.arange(WIN_COLS, dtype=jnp.int32)[:, None]
    )
    inside = (offsets >= 0) & (offsets < WIN_COLS)
    one_hot = (offsets[:, :, None] == jnp.arange(WIN_COLS, dtype=jnp.int32)[None, None, :]).astype(
        jnp.float32
    )
    lookup = jnp.einsum("hjc,qkc->qhjk", head_bias, one_hot, precision=lax.Precision.HIGHEST)
    return (lookup, inside)


def window_attend(queries, pair_pad, query_marks, mark_pad, head_bias):
    heads_here = head_bias.shape[0]
    tokens_here = queries.shape[0]
    grid_rows = tokens_here // GRID_W
    col_blocks = GRID_W // WIN_COLS
    key_reach = 2 * WIN_COLS - 1
    margin = WIN_COLS // 2
    col_pad = ((0, 0), (margin, WIN_COLS - 1 - margin))
    pair_grid = jnp.pad(pair_pad.reshape(grid_rows + WIN_ROWS, GRID_W, -1), col_pad + ((0, 0),))
    mark_grid = jnp.pad(mark_pad.reshape(grid_rows + WIN_ROWS, GRID_W), col_pad)
    pair_band = jnp.stack(
        [pair_grid[row_shift : row_shift + grid_rows] for row_shift in range(WIN_ROWS)], axis=1
    )
    mark_band = jnp.stack(
        [mark_grid[row_shift : row_shift + grid_rows] for row_shift in range(WIN_ROWS)], axis=1
    )
    pair_win = jnp.stack(
        [
            pair_band[:, :, col_block * WIN_COLS : col_block * WIN_COLS + key_reach]
            for col_block in range(col_blocks)
        ],
        axis=2,
    )
    mark_win = jnp.stack(
        [
            mark_band[:, :, col_block * WIN_COLS : col_block * WIN_COLS + key_reach]
            for col_block in range(col_blocks)
        ],
        axis=2,
    )
    pair_win = pair_win.reshape(grid_rows, WIN_ROWS, col_blocks, key_reach, 2, heads_here, HEAD_DIM)
    key_win = pair_win[:, :, :, :, 0]
    value_win = pair_win[:, :, :, :, 1]
    query_grid = queries.reshape(grid_rows, col_blocks, WIN_COLS, heads_here, HEAD_DIM)
    scores = jnp.einsum(
        "rbqhd,rjbkhd->rbqhjk", query_grid, key_win, preferred_element_type=jnp.float32
    )
    lookup, inside = offset_table(head_bias)
    own_marks = query_marks.reshape(grid_rows, col_blocks, WIN_COLS)
    same_doc = mark_win.transpose(0, 2, 1, 3)[:, :, None, :, :] == own_marks[:, :, :, None, None]
    allowed = same_doc & inside[None, None, :, None, :]
    scores = scores * HEAD_DIM ** (-0.5) + lookup[None, None]
    scores = jnp.where(allowed[:, :, :, None], scores, -jnp.inf)
    highest = jnp.max(scores, axis=(4, 5), keepdims=True)
    shifted_exp = jnp.exp(scores - highest)
    weights = (shifted_exp / jnp.sum(shifted_exp, axis=(4, 5), keepdims=True)).astype(jnp.bfloat16)
    mixed = jnp.einsum(
        "rbqhjk,rjbkhd->rbqhd", weights, value_win, preferred_element_type=jnp.float32
    )
    return mixed.astype(jnp.bfloat16).reshape(tokens_here, heads_here * HEAD_DIM)


def attend(projected, marks, head_bias):
    head_width = projected.shape[1] // 3
    halo_tokens = WIN_ROWS // 2 * GRID_W
    pair_pad, mark_pad = (
        padded(projected[:, head_width:], (("sp", 0),), halo_tokens),
        padded(marks, (("sp", 0),), halo_tokens),
    )
    return window_attend(projected[:, :head_width], pair_pad, marks, mark_pad, head_bias)


def on_device(
    stream, doc_ids, norm_gain, w_query, w_key, w_value, query_gain, key_gain, offset_bias, w_output
):
    marks = (doc_ids + 1).astype(jnp.bfloat16)
    layer_count = w_query.shape[0]
    current = stream
    for layer_index in range(layer_count):
        layer_params = (
            norm_gain[layer_index],
            w_query[layer_index],
            w_key[layer_index],
            w_value[layer_index],
            query_gain[layer_index],
            key_gain[layer_index],
        )
        attended = attend(project(layer_params, current), marks, offset_bias[layer_index])
        every_head = lax.all_gather(attended, "tp", axis=1, tiled=True)
        projected = jnp.dot(every_head, w_output[layer_index], preferred_element_type=jnp.float32)
        current = (current.astype(jnp.float32) + projected).astype(jnp.bfloat16)
    return current


def solution(mesh):
    return jax.shard_map(
        on_device,
        mesh=mesh,
        in_specs=(
            P("sp", None),
            P("sp"),
            P(),
            P(None, None, "tp"),
            P(None, None, "tp"),
            P(None, None, "tp"),
            P(),
            P(),
            P(None, "tp", None, None),
            P(),
        ),
        out_specs=P("sp", None),
        check_vma=False,
    )
```

profile of v0, /device:TPU:6, one launch (start us, length us, event | category | flops | bytes accessed | tf_op | source)
XLA Modules:
  0.0 237.8 jit_solution(1758482249919251222)
XLA Ops:
  0.8 1.5 fusion.38
  2.3 3.9 %slice_bitcast_fusion.9 = (bf16[512,2048]{0,1:T(8,128)(2,1)S(1)}, bf16[512,2048]{0,1:T(8,128)(2,1)}) fusion(bf16[2,2048,512]{2,1,0:T(8,128)(2,1)} %param.14), kind=kLoop, calls=%fused_computation.66 | loop fusion | bytes 8388608 | tf_op jit(solution)/shard_map/dot_general | solution.py:42
  6.2 4.0 %copy.68 = bf16[512,2048]{1,0:T(8,128)(2,1)} copy(bf16[512,2048]{0,1:T(8,128)(2,1)} %get-tuple-element.16) | data formatting | bytes 4194304 | tf_op jit(solution)/shard_map/dot_general | solution.py:42
  10.2 2.4 %multiply_reduce_fusion.3 = (f32[256,8]{0,1:T(8,128)S(1)}, f32[256,8,64]{0,2,1:T(8,128)S(1)}) fusion(bf16[8,64,2048]{2,1,0:T(8,128)(2,1)} %bitcast.333, f32[2048]{0:T(1024)S(1)} %bitcast.341, f32[256]{0:T(256)S(1)} %add_rsqrt_fusion.5, bf16[256,2048]{1,0:T(8,128)(2,1)S(1)} %copy-done.8), kind=kOutput, calls=%fused_computation.150 | convolution fusion | flops 539228160 | bytes 3687424 | tf_op jit(solution)/shard_map/dot_general | solution.py:42
  13.0 2.8 %fusion.56 = bf16[256,512]{1,0:T(8,128)(2,1)S(1)} fusion(bf16[2,2048,512]{2,1,0:T(8,128)(2,1)} %param.15, bf16[256,2048]{1,0:T(8,128)(2,1)} %param.10, f32[2048]{0:T(1024)S(1)} %bitcast.342, f32[256]{0:T(256)S(1)} %add_rsqrt_fusion.5), kind=kOutput, calls=%fused_computation.96 | convolution fusion | flops 539099136 | bytes 3417088 | tf_op jit(solution)/shard_map/dot_general | solution.py:43
  16.7 1.9 collective-permute-start
  18.6 3.6 %collective-permute-start.1 = (bf16[256,1024]{1,0:T(8,128)(2,1)}, bf16[256,1024]{1,0:T(8,128)(2,1)}, u32[]{:S(2)}, u32[]{:S(2)}) collective-permute-start(bf16[256,1024]{1,0:T(8,128)(2,1)} %pad_maximum_fusion.2), channel_id=1, source_target_pairs={{2,0},{4,2},{6,4},{8,6},{10,8},{12,10},{14,12},{16,14},{18,16},{20... | collective-permute-start | bytes 1572872 | tf_op jit(solution)/shard_map/ppermute | solution.py:23
  22.3 1.9 collective-permute-start.2
  24.2 3.6 %collective-permute-start.3 = (bf16[256]{0:T(256)(128)(2,1)S(1)}, bf16[256]{0:T(256)(128)(2,1)S(1)}, u32[]{:S(2)}, u32[]{:S(2)}) collective-permute-start(bf16[256]{0:T(256)(128)(2,1)S(1)} %add_convert_fusion), channel_id=1, source_target_pairs={{2,0},{4,2},{6,4},{8,6},{10,8},{12,10},{14,12},{16,14},{18,16},{20... | collective-permute-start | bytes 1544 | tf_op jit(solution)/shard_map/ppermute | solution.py:23
  29.4 2.2 slice_bitcast_fusion.8
  31.6 4.2 %copy.79 = bf16[512,2048]{1,0:T(8,128)(2,1)} copy(bf16[512,2048]{0,1:T(8,128)(2,1)} %get-tuple-element.14) | data formatting | bytes 4194304 | tf_op jit(solution)/shard_map/dot_general | solution.py:40
  35.8 2.8 %multiply_reduce_fusion.2 = (f32[256,8]{0,1:T(8,128)S(1)}, f32[256,8,64]{0,2,1:T(8,128)S(1)}) fusion(bf16[8,64,2048]{2,1,0:T(8,128)(2,1)} %bitcast.332, f32[2048]{0:T(1024)S(1)} %bitcast.343, f32[256]{0:T(256)S(1)} %add_rsqrt_fusion.5, bf16[256,2048]{1,0:T(8,128)(2,1)} %param.10), kind=kOutput, calls=%fused_computation.148 | convolution fusion | flops 539228160 | bytes 3687424 | tf_op jit(solution)/shard_map/dot_general | solution.py:40
  41.1 2.5 %copy.84 = bf16[512,2048]{1,0:T(8,128)(2,1)} copy(bf16[512,2048]{0,1:T(8,128)(2,1)S(1)} %get-tuple-element.15) | data formatting | bytes 4194304 | tf_op jit(solution)/shard_map/dot_general | solution.py:42
  43.5 4.0 %copy.94 = bf16[512,2048]{1,0:T(8,128)(2,1)} copy(bf16[512,2048]{0,1:T(8,128)(2,1)} %get-tuple-element.13) | data formatting | bytes 4194304 | tf_op jit(solution)/shard_map/dot_general | solution.py:40
  48.7 1.3 pad_maximum_fusion
  50.6 3.0 %fusion.130 = (bf16[4,8,31,1024]{3,2,0,1:T(8,128)(2,1)S(1)}, bf16[4,8,31,1024]{3,2,0,1:T(8,128)(2,1)}, bf16[4,8,31,1024]{3,2,0,1:T(8,128)(2,1)}, bf16[4,8,31,1024]{3,2,0,1:T(8,128)(2,1)}) fusion(bf16[4,8,79,1024]{3,2,0,1:T(8,128)(2,1)S(1)} %fusion.85), kind=kLoop, calls=%fused_computation.206 | loop fusion | bytes 16252928 | tf_op jit(solution)/shard_map/slice | solution.py:81
  53.6 6.2 %reshape.154 = bf16[4,8,1,31,2,8,64]{6,5,4,3,0,1,2:T(8,128)(2,1)} reshape(bf16[4,8,31,1024]{3,2,0,1:T(8,128)(2,1)} %get-tuple-element.12) | data formatting | bytes 4063232 | tf_op jit(solution)/shard_map/stack | solution.py:79
  59.8 5.2 %copy_dynamic-update-slice_fusion.7 = bf16[4,8,4,31,2,8,64]{6,3,1,5,2,0,4:T(8,128)(2,1)} fusion(bf16[4,8,1,31,2,8,64]{6,5,4,3,0,1,2:T(8,128)(2,1)} %reshape.154), kind=kLoop, calls=%fused_computation.31 | loop fusion | bytes 6225920
  65.0 6.2 %reshape.155 = bf16[4,8,1,31,2,8,64]{6,5,4,3,0,1,2:T(8,128)(2,1)} reshape(bf16[4,8,31,1024]{3,2,0,1:T(8,128)(2,1)} %get-tuple-element.11) | data formatting | bytes 4063232 | tf_op jit(solution)/shard_map/stack | solution.py:79
  71.1 6.2 %reshape.156 = bf16[4,8,1,31,2,8,64]{6,5,4,3,0,1,2:T(8,128)(2,1)} reshape(bf16[4,8,31,1024]{3,2,0,1:T(8,128)(2,1)} %get-tuple-element.10) | data formatting | bytes 4063232 | tf_op jit(solution)/shard_map/stack | solution.py:79
  77.4 3.9 %reshape.157 = bf16[4,8,1,31,2,8,64]{6,5,4,3,0,1,2:T(8,128)(2,1)} reshape(bf16[4,8,31,1024]{3,2,0,1:T(8,128)(2,1)S(1)} %get-tuple-element.9) | data formatting | bytes 4063232 | tf_op jit(solution)/shard_map/stack | solution.py:79
  81.2 5.3 %copy_dynamic-update-slice_fusion.6 = bf16[4,8,4,31,2,8,64]{6,3,1,5,2,0,4:T(8,128)(2,1)} fusion(bf16[4,8,4,31,2,8,64]{6,3,1,5,2,0,4:T(8,128)(2,1)} %copy_dynamic-update-slice_fusion.7, bf16[4,8,1,31,2,8,64]{6,5,4,3,0,1,2:T(8,128)(2,1)} %reshape.155), kind=kLoop, calls=%fused_computation.30 | loop fusion | bytes 8257536
  86.6 3.0 %copy_dynamic-update-slice_fusion.5 = bf16[4,8,4,31,2,8,64]{6,3,1,5,2,0,4:T(8,128)(2,1)} fusion(bf16[4,8,4,31,2,8,64]{6,3,1,5,2,0,4:T(8,128)(2,1)} %copy_dynamic-update-slice_fusion.6, bf16[4,8,1,31,2,8,64]{6,5,4,3,0,1,2:T(8,128)(2,1)S(1)} %copy-done), kind=kLoop, calls=%fused_computation.29 | loop fusion | bytes 6225920
  89.6 3.0 %copy_dynamic-update-slice_fusion.4 = bf16[4,8,4,31,2,8,64]{6,3,1,5,2,0,4:T(8,128)(2,1)} fusion(bf16[4,8,4,31,2,8,64]{6,3,1,5,2,0,4:T(8,128)(2,1)} %copy_dynamic-update-slice_fusion.5, bf16[4,8,1,31,2,8,64]{6,5,4,3,0,1,2:T(8,128)(2,1)S(1)} %copy-done.1), kind=kLoop, calls=%fused_computation.28 | loop fusion | bytes 6225920 | tf_op jit(solution)/shard_map/stack | solution.py:79
  92.6 13.9 %fusion.8 = (f32[4,4,16,8]{2,3,1,0:T(8,128)S(1)}, f32[4,4,8,8,31,16]{4,5,3,2,1,0:T(8,128)S(1)}) fusion(f32[16,8,8,31]{3,0,2,1:T(8,128)} %copy.82, pred[4,4,16,8,31]{4,2,3,1,0:T(8,128)(4,1)S(1)} %compare_and_fusion, bf16[4,4,16,8,64,1]{4,3,2,1,0,5:T(8,128)(2,1)} %bitcast.336, bf16[4,8,4,31,2,8,64]{6,3,1,5,2,0,4:T(8,128)(2,1)} %copy_dynamic-update-slice_fusion.4), kind=kOutput, calls=%fused_computation.18 | convolution fusion | flops 67041280 | bytes 11540480 | tf_op jit(solution)/shard_map/rbqhd,rjbkhd->rbqhjk/dot_general | solution.py:97
  106.5 3.9 %fusion.6 = f32[4,4,16,8]{2,3,1,0:T(8,128)S(1)} fusion(f32[4,4,8,8,31,16]{4,5,3,2,1,0:T(8,128)S(1)} %get-tuple-element.32, f32[4,4,16,8]{2,3,1,0:T(8,128)S(1)} %get-tuple-element.31, f32[16,8,8,31]{3,0,2,1:T(8,128)} %copy.82, pred[4,4,16,8,31]{4,2,3,1,0:T(8,128)(4,1)S(1)} %compare_and_fusion), kind=kLoop, calls=%fused_computation.16 | loop fusion | flops 2537472 | bytes 2238464 | tf_op jit(solution)/shard_map/reduce_sum | solution.py:108
  110.5 10.3 %fusion.54 = bf16[4,4,16,8,64]{4,2,3,1,0:T(8,128)(2,1)S(1)} fusion(f32[4,4,8,8,31,16]{4,5,3,2,1,0:T(8,128)S(1)} %get-tuple-element.32, f32[4,4,16,8]{2,3,1,0:T(8,128)S(1)} %fusion.6, f32[4,4,16,8]{2,3,1,0:T(8,128)S(1)} %get-tuple-element.31, f32[16,8,8,31]{3,0,2,1:T(8,128)S(1)} %copy-done.5, pred[4,4,16,8,31]{4,2,3,1,0:T(8,128)(4,1)S(1)} %compare_and_fusion, ...), kind=kOutput, calls=%fused_computation.94 | convolution fusion | flops 68190208 | bytes 10889216 | tf_op jit(solution)/shard_map/rbqhjk,rjbkhd->rbqhd/dot_general | solution.py:109
  121.2 9.7 %all_gather.6 = bf16[256,1024]{1,0:T(8,128)(2,1)S(1)} all-gather(bf16[256,512]{1,0:T(8,128)(2,1)S(1)} %reshape.141), channel_id=1, replica_groups=mesh['sp'=16,'tp'=2] {'tp'}, dimensions={1}, use_global_device_ids=true | all-gather | bytes 786432 | tf_op jit(solution)/shard_map/all_gather | solution.py:141
  131.0 4.1 %fusion.41 = (f32[256]{0:T(256)S(1)}, bf16[256,2048]{1,0:T(8,128)(2,1)S(1)}) fusion(bf16[256,1024]{1,0:T(8,128)(2,1)S(1)} %all_gather.6, bf16[2,1024,2048]{2,1,0:T(8,128)(2,1)} %param.19, bf16[256,2048]{1,0:T(8,128)(2,1)} %param.10), kind=kOutput, calls=%fused_computation.57 | convolution fusion | flops 1076887296 | bytes 6816768 | tf_op jit(solution)/shard_map/dot_general | solution.py:142
  138.2 1.9 collective-permute-start.4
  140.1 3.6 %collective-permute-start.5 = (bf16[256,1024]{1,0:T(8,128)(2,1)S(1)}, bf16[256,1024]{1,0:T(8,128)(2,1)}, u32[]{:S(2)}, u32[]{:S(2)}) collective-permute-start(bf16[256,1024]{1,0:T(8,128)(2,1)S(1)} %pad_maximum_fusion.3), channel_id=1, source_target_pairs={{2,0},{4,2},{6,4},{8,6},{10,8},{12,10},{14,12},{16,14},{18,16},{20... | collective-permute-start | bytes 1572872 | tf_op jit(solution)/shard_map/ppermute | solution.py:23
  143.8 2.8 %multiply_reduce_fusion = (f32[256,8]{0,1:T(8,128)S(1)}, f32[256,8,64]{0,2,1:T(8,128)S(1)}) fusion(bf16[8,64,2048]{2,1,0:T(8,128)(2,1)} %bitcast.330, f32[2048]{0:T(1024)S(1)} %bitcast.340, f32[256]{0:T(256)S(1)} %add_rsqrt_fusion.4, bf16[256,2048]{1,0:T(8,128)(2,1)} %copy-done.14), kind=kOutput, calls=%fused_computation.144 | convolution fusion | flops 539228160 | bytes 3687424 | tf_op jit(solution)/shard_map/dot_general | solution.py:40
  147.8 6.6 %collective-permute-done.4 = bf16[256,1024]{1,0:T(8,128)(2,1)S(1)} collective-permute-done((bf16[256,1024]{1,0:T(8,128)(2,1)S(1)}, bf16[256,1024]{1,0:T(8,128)(2,1)S(1)}, u32[]{:S(2)}, u32[]{:S(2)}) %collective-permute-start.4) | collective-permute-done | bytes 524320 | tf_op jit(solution)/shard_map/ppermute | solution.py:20
  154.3 1.2 pad_maximum_fusion.1
  156.1 3.3 %fusion.129 = (bf16[4,8,31,1024]{3,2,0,1:T(8,128)(2,1)S(1)}, bf16[4,8,31,1024]{3,2,0,1:T(8,128)(2,1)}, bf16[4,8,31,1024]{3,2,0,1:T(8,128)(2,1)}, bf16[4,8,31,1024]{3,2,0,1:T(8,128)(2,1)}) fusion(bf16[4,8,79,1024]{3,2,0,1:T(8,128)(2,1)S(1)} %fusion.101), kind=kLoop, calls=%fused_computation.205 | loop fusion | bytes 16252928 | tf_op jit(solution)/shard_map/slice | solution.py:81
  159.4 6.2 %reshape.158 = bf16[4,8,1,31,2,8,64]{6,5,4,3,0,1,2:T(8,128)(2,1)} reshape(bf16[4,8,31,1024]{3,2,0,1:T(8,128)(2,1)} %get-tuple-element.8) | data formatting | bytes 4063232 | tf_op jit(solution)/shard_map/stack | solution.py:79
  165.6 5.2 %copy_dynamic-update-slice_fusion.3 = bf16[4,8,4,31,2,8,64]{6,3,1,5,2,0,4:T(8,128)(2,1)} fusion(bf16[4,8,1,31,2,8,64]{6,5,4,3,0,1,2:T(8,128)(2,1)} %reshape.158), kind=kLoop, calls=%fused_computation.25 | loop fusion | bytes 6225920
  170.8 6.2 %reshape.159 = bf16[4,8,1,31,2,8,64]{6,5,4,3,0,1,2:T(8,128)(2,1)} reshape(bf16[4,8,31,1024]{3,2,0,1:T(8,128)(2,1)} %get-tuple-element.7) | data formatting | bytes 4063232 | tf_op jit(solution)/shard_map/stack | solution.py:79
  177.0 6.2 %reshape.160 = bf16[4,8,1,31,2,8,64]{6,5,4,3,0,1,2:T(8,128)(2,1)} reshape(bf16[4,8,31,1024]{3,2,0,1:T(8,128)(2,1)} %get-tuple-element.6) | data formatting | bytes 4063232 | tf_op jit(solution)/shard_map/stack | solution.py:79
  183.2 3.9 %reshape.161 = bf16[4,8,1,31,2,8,64]{6,5,4,3,0,1,2:T(8,128)(2,1)} reshape(bf16[4,8,31,1024]{3,2,0,1:T(8,128)(2,1)S(1)} %get-tuple-element.5) | data formatting | bytes 4063232 | tf_op jit(solution)/shard_map/stack | solution.py:79
  187.1 5.3 %copy_dynamic-update-slice_fusion.2 = bf16[4,8,4,31,2,8,64]{6,3,1,5,2,0,4:T(8,128)(2,1)} fusion(bf16[4,8,4,31,2,8,64]{6,3,1,5,2,0,4:T(8,128)(2,1)} %copy_dynamic-update-slice_fusion.3, bf16[4,8,1,31,2,8,64]{6,5,4,3,0,1,2:T(8,128)(2,1)} %reshape.159), kind=kLoop, calls=%fused_computation.24 | loop fusion | bytes 8257536
  192.4 3.0 %copy_dynamic-update-slice_fusion.1 = bf16[4,8,4,31,2,8,64]{6,3,1,5,2,0,4:T(8,128)(2,1)} fusion(bf16[4,8,4,31,2,8,64]{6,3,1,5,2,0,4:T(8,128)(2,1)} %copy_dynamic-update-slice_fusion.2, bf16[4,8,1,31,2,8,64]{6,5,4,3,0,1,2:T(8,128)(2,1)S(1)} %copy-done.2), kind=kLoop, calls=%fused_computation.23 | loop fusion | bytes 6225920
  195.4 3.0 %copy_dynamic-update-slice_fusion = bf16[4,8,4,31,2,8,64]{6,3,1,5,2,0,4:T(8,128)(2,1)} fusion(bf16[4,8,4,31,2,8,64]{6,3,1,5,2,0,4:T(8,128)(2,1)} %copy_dynamic-update-slice_fusion.1, bf16[4,8,1,31,2,8,64]{6,5,4,3,0,1,2:T(8,128)(2,1)S(1)} %copy-done.3), kind=kLoop, calls=%fused_computation.22 | loop fusion | bytes 6225920 | tf_op jit(solution)/shard_map/stack | solution.py:79
  198.4 13.6 %fusion.9 = (f32[4,4,16,8]{2,3,1,0:T(8,128)S(1)}, f32[4,4,8,8,31,16]{4,5,3,2,1,0:T(8,128)S(1)}) fusion(f32[16,8,8,31]{3,0,2,1:T(8,128)S(1)} %copy.97, pred[4,4,16,8,31]{4,2,3,1,0:T(8,128)(4,1)S(1)} %compare_and_fusion, bf16[4,4,16,8,64,1]{4,3,2,1,0,5:T(8,128)(2,1)} %bitcast.337, bf16[4,8,4,31,2,8,64]{6,3,1,5,2,0,4:T(8,128)(2,1)} %copy_dynamic-update-slice_fusion), kind=kOutput, calls=%fused_computation.19 | convolution fusion | flops 67041280 | bytes 11143168 | tf_op jit(solution)/shard_map/rbqhd,rjbkhd->rbqhjk/dot_general | solution.py:97
  212.1 3.0 %fusion.7 = f32[4,4,16,8]{2,3,1,0:T(8,128)S(1)} fusion(f32[4,4,8,8,31,16]{4,5,3,2,1,0:T(8,128)S(1)} %get-tuple-element.40, f32[4,4,16,8]{2,3,1,0:T(8,128)S(1)} %get-tuple-element.39, f32[16,8,8,31]{3,0,2,1:T(8,128)S(1)} %copy.97, pred[4,4,16,8,31]{4,2,3,1,0:T(8,128)(4,1)S(1)} %compare_and_fusion), kind=kLoop, calls=%fused_computation.17 | loop fusion | flops 2537472 | bytes 2238464 | tf_op jit(solution)/shard_map/reduce_sum | solution.py:108
  215.1 10.3 %fusion.55 = bf16[4,4,16,8,64]{4,2,3,1,0:T(8,128)(2,1)S(1)} fusion(f32[4,4,8,8,31,16]{4,5,3,2,1,0:T(8,128)S(1)} %get-tuple-element.40, f32[4,4,16,8]{2,3,1,0:T(8,128)S(1)} %fusion.7, f32[4,4,16,8]{2,3,1,0:T(8,128)S(1)} %get-tuple-element.39, f32[16,8,8,31]{3,0,2,1:T(8,128)S(1)} %copy.97, pred[4,4,16,8,31]{4,2,3,1,0:T(8,128)(4,1)S(1)} %compare_and_fusion, ...), kind=kOutput, calls=%fused_computation.95 | convolution fusion | flops 68190208 | bytes 10889216 | tf_op jit(solution)/shard_map/rbqhjk,rjbkhd->rbqhd/dot_general | solution.py:109
  225.9 7.1 %all_gather.7 = bf16[256,1024]{1,0:T(8,128)(2,1)S(1)} all-gather(bf16[256,512]{1,0:T(8,128)(2,1)S(1)} %reshape.144), channel_id=1, replica_groups=mesh['sp'=16,'tp'=2] {'tp'}, dimensions={1}, use_global_device_ids=true | all-gather | bytes 786432 | tf_op jit(solution)/shard_map/all_gather | solution.py:141
  232.9 4.7 %fusion.35 = bf16[256,2048]{1,0:T(8,128)(2,1)} fusion(bf16[256,1024]{1,0:T(8,128)(2,1)S(1)} %all_gather.7, bf16[2,1024,2048]{2,1,0:T(8,128)(2,1)} %param.19, bf16[256,2048]{1,0:T(8,128)(2,1)} %copy-done.14), kind=kOutput, calls=%fused_computation.53 | convolution fusion | flops 1075314688 | bytes 6815744 | tf_op jit(solution)/shard_map/dot_general | solution.py:142
  (100 shorter events, 13.3 us)
Async XLA Ops:
  6.2 4.0 %copy-start.8 = (bf16[256,2048]{1,0:T(8,128)(2,1)S(1)}, bf16[256,2048]{1,0:T(8,128)(2,1)}, u32[]{:S(2)}) copy-start(bf16[256,2048]{1,0:T(8,128)(2,1)} %param.10) | copy-start | bytes 3145732
  6.2 6.5 %copy-start.10 = (f32[2,64]{1,0:T(2,128)S(1)}, f32[2,64]{1,0:T(2,128)}, u32[]{:S(2)}) copy-start(f32[2,64]{1,0:T(2,128)} %param.17) | copy-start | bytes 1540
  12.7 9.6 %copy-start.13 = (s32[256]{0:T(256)S(1)}, s32[256]{0:T(256)}, u32[]{:S(2)}) copy-start(s32[256]{0:T(256)} %param.11) | copy-start | bytes 3076
  12.7 15.2 %copy-start.9 = (f32[2,8,8,16]{3,2,1,0:T(8,128)S(1)}, f32[2,8,8,16]{3,2,1,0:T(8,128)}, u32[]{:S(2)}) copy-start(f32[2,8,8,16]{3,2,1,0:T(8,128)} %param.18) | copy-start | bytes 24580
  13.0 16.4 %copy-start.4 = (bf16[2,2048,512]{2,1,0:T(8,128)(2,1)S(1)}, bf16[2,2048,512]{2,1,0:T(8,128)(2,1)}, u32[]{:S(2)}) copy-start(bf16[2,2048,512]{2,1,0:T(8,128)(2,1)} %param.13) | copy-start | bytes 12582916
  16.7 32.0 %collective-permute-start = (bf16[256,1024]{1,0:T(8,128)(2,1)}, bf16[256,1024]{1,0:T(8,128)(2,1)}, u32[]{:S(2)}, u32[]{:S(2)}) collective-permute-start(bf16[256,1024]{1,0:T(8,128)(2,1)} %pad_maximum_fusion.2), channel_id=1, source_target_pairs={{0,2},{2,4},{4,6},{6,8},{8,10},{10,12},{12,14},{14,16},{16,18},{18... | collective-permute-start | bytes 1572872 | tf_op jit(solution)/shard_map/ppermute | solution.py:20
  18.6 30.1 %collective-permute-start.1 = (bf16[256,1024]{1,0:T(8,128)(2,1)}, bf16[256,1024]{1,0:T(8,128)(2,1)}, u32[]{:S(2)}, u32[]{:S(2)}) collective-permute-start(bf16[256,1024]{1,0:T(8,128)(2,1)} %pad_maximum_fusion.2), channel_id=1, source_target_pairs={{2,0},{4,2},{6,4},{8,6},{10,8},{12,10},{14,12},{16,14},{18,16},{20... | collective-permute-start | bytes 1572872 | tf_op jit(solution)/shard_map/ppermute | solution.py:23
  22.3 25.6 %collective-permute-start.2 = (bf16[256]{0:T(256)(128)(2,1)S(1)}, bf16[256]{0:T(256)(128)(2,1)S(1)}, u32[]{:S(2)}, u32[]{:S(2)}) collective-permute-start(bf16[256]{0:T(256)(128)(2,1)S(1)} %add_convert_fusion), channel_id=1, source_target_pairs={{0,2},{2,4},{4,6},{6,8},{8,10},{10,12},{12,14},{14,16},{16,18},{18... | collective-permute-start | bytes 1544 | tf_op jit(solution)/shard_map/ppermute | solution.py:20
  24.2 23.7 %collective-permute-start.3 = (bf16[256]{0:T(256)(128)(2,1)S(1)}, bf16[256]{0:T(256)(128)(2,1)S(1)}, u32[]{:S(2)}, u32[]{:S(2)}) collective-permute-start(bf16[256]{0:T(256)(128)(2,1)S(1)} %add_convert_fusion), channel_id=1, source_target_pairs={{2,0},{4,2},{6,4},{8,6},{10,8},{12,10},{14,12},{16,14},{18,16},{20... | collective-permute-start | bytes 1544 | tf_op jit(solution)/shard_map/ppermute | solution.py:23
  31.6 6.9 %copy-start.11 = (f32[2,64]{1,0:T(2,128)S(1)}, f32[2,64]{1,0:T(2,128)}, u32[]{:S(2)}) copy-start(f32[2,64]{1,0:T(2,128)} %param.16) | copy-start | bytes 1540
  43.5 4.0 %copy-start.7 = (f32[16,8,8,31]{3,2,1,0:T(8,128)S(1)}, f32[16,8,8,31]{3,2,1,0:T(8,128)}, u32[]{:S(2)}) copy-start(f32[16,8,8,31]{3,2,1,0:T(8,128)} %convolution_bitcast_fusion) | copy-start | bytes 380932
  81.2 5.3 %copy-start = (bf16[4,8,1,31,2,8,64]{6,5,4,3,0,1,2:T(8,128)(2,1)S(1)}, bf16[4,8,1,31,2,8,64]{6,5,4,3,0,1,2:T(8,128)(2,1)}, u32[]{:S(2)}) copy-start(bf16[4,8,1,31,2,8,64]{6,5,4,3,0,1,2:T(8,128)(2,1)} %reshape.156) | copy-start | bytes 6094852
  86.6 3.0 %copy-start.1 = (bf16[4,8,1,31,2,8,64]{6,5,4,3,0,1,2:T(8,128)(2,1)S(1)}, bf16[4,8,1,31,2,8,64]{6,5,4,3,0,1,2:T(8,128)(2,1)}, u32[]{:S(2)}) copy-start(bf16[4,8,1,31,2,8,64]{6,5,4,3,0,1,2:T(8,128)(2,1)} %reshape.157) | copy-start | bytes 6094852
  106.5 3.9 %copy-start.5 = (f32[16,8,8,31]{3,0,2,1:T(8,128)S(1)}, f32[16,8,8,31]{3,0,2,1:T(8,128)}, u32[]{:S(2)}) copy-start(f32[16,8,8,31]{3,0,2,1:T(8,128)} %copy.82) | copy-start | bytes 380932
  131.0 4.1 %copy-start.12 = (bf16[2,2048,512]{2,1,0:T(8,128)(2,1)S(1)}, bf16[2,2048,512]{2,1,0:T(8,128)(2,1)}, u32[]{:S(2)}) copy-start(bf16[2,2048,512]{2,1,0:T(8,128)(2,1)} %param.15) | copy-start | bytes 12582916
  135.0 2.8 %copy-start.14 = (bf16[256,2048]{1,0:T(8,128)(2,1)}, bf16[256,2048]{1,0:T(8,128)(2,1)S(1)}, u32[]{:S(2)}) copy-start(bf16[256,2048]{1,0:T(8,128)(2,1)S(1)} %get-tuple-element.34) | copy-start | bytes 3145732
  135.0 2.0 copy-start.6
  138.2 16.1 %collective-permute-start.4 = (bf16[256,1024]{1,0:T(8,128)(2,1)S(1)}, bf16[256,1024]{1,0:T(8,128)(2,1)S(1)}, u32[]{:S(2)}, u32[]{:S(2)}) collective-permute-start(bf16[256,1024]{1,0:T(8,128)(2,1)S(1)} %pad_maximum_fusion.3), channel_id=1, source_target_pairs={{0,2},{2,4},{4,6},{6,8},{8,10},{10,12},{12,14},{14,16},{16,18},{18... | collective-permute-start | bytes 1572872 | tf_op jit(solution)/shard_map/ppermute | solution.py:20
  140.1 14.2 %collective-permute-start.5 = (bf16[256,1024]{1,0:T(8,128)(2,1)S(1)}, bf16[256,1024]{1,0:T(8,128)(2,1)}, u32[]{:S(2)}, u32[]{:S(2)}) collective-permute-start(bf16[256,1024]{1,0:T(8,128)(2,1)S(1)} %pad_maximum_fusion.3), channel_id=1, source_target_pairs={{2,0},{4,2},{6,4},{8,6},{10,8},{12,10},{14,12},{16,14},{18,16},{20... | collective-permute-start | bytes 1572872 | tf_op jit(solution)/shard_map/ppermute | solution.py:23
  187.1 5.3 %copy-start.2 = (bf16[4,8,1,31,2,8,64]{6,5,4,3,0,1,2:T(8,128)(2,1)S(1)}, bf16[4,8,1,31,2,8,64]{6,5,4,3,0,1,2:T(8,128)(2,1)}, u32[]{:S(2)}) copy-start(bf16[4,8,1,31,2,8,64]{6,5,4,3,0,1,2:T(8,128)(2,1)} %reshape.160) | copy-start | bytes 6094852
  192.4 3.0 %copy-start.3 = (bf16[4,8,1,31,2,8,64]{6,5,4,3,0,1,2:T(8,128)(2,1)S(1)}, bf16[4,8,1,31,2,8,64]{6,5,4,3,0,1,2:T(8,128)(2,1)}, u32[]{:S(2)}) copy-start(bf16[4,8,1,31,2,8,64]{6,5,4,3,0,1,2:T(8,128)(2,1)} %reshape.161) | copy-start | bytes 6094852
where the time goes:
time: 243 us; the launch traced here: 238 us
  local copies, waits for them, and re-layouts  113 us (47%)
  matrix products  70.8 us (29%)
  blocking collectives  16.8 us (7%)
  starting transfers between devices  16.7 us (7%)
  other arithmetic  12.8 us (5%)
  waiting for transfers between devices  6.59 us (3%)
    another operation x10, local copies, waits for them, and re-layouts, window_attend(): jnp.stack([pair_band[:, :, col_block * WIN_COLS:col_block * WIN_COLS + ke...  51 us
    unnamed x57, local copies, waits for them, and re-layouts  29.3 us
    dot_general x2, matrix products, window_attend(): jnp.einsum('rbqhd,rjbkhd->rbqhjk', query_grid, key_win, preferred_element...  27.5 us
    dot_general x2, matrix products, window_attend(): jnp.einsum('rbqhjk,rjbkhd->rbqhd', weights, value_win, preferred_element_...  20.6 us
    all_gather x2, blocking collectives, on_device(): every_head = lax.all_gather(attended, 'tp', axis=1, tiled=True)  16.8 us
    ppermute x3, starting transfers between devices, padded(): lax.ppermute(lax.slice_in_dim(block, 0, width, axis=dim), axis, backward)  10.9 us
    dot_general x3, local copies, waits for them, and re-layouts, project(): jnp.dot(normed, query_weight, preferred_element_type=jnp.float32)  10.4 us
    dot_general x3, local copies, waits for them, and re-layouts, project(): jnp.dot(normed, key_weight, preferred_element_type=jnp.float32)  10.3 us
  transfers between devices with their start and end apart: 6, of which 1 were waited for; matrix products, arithmetic and copies ran while one was open for 10% of the time, Pallas kernels for 0%

commit v1 on v0

v1 whole, which is shorter than its diff:
```python
import functools

import jax
import jax.numpy as jnp
from jax import lax
from jax.experimental import pallas as pl
from jax.experimental.pallas import tpu as pltpu
from jax.sharding import PartitionSpec as P

HEAD_DIM = 64
GRID_W = 64
WIN_ROWS = 8
WIN_COLS = 16
ROWS_UP = WIN_ROWS // 2
ROWS_DOWN = WIN_ROWS - 1 - ROWS_UP
LANES = 128
MARK_ROWS = 16
WINDOW = WIN_ROWS * GRID_W
FAR = -1e30
EPS = 1e-06
VMEM_LIMIT = 28 << 20

bf16, f32 = jnp.bfloat16, jnp.float32
VMEM = pl.BlockSpec(memory_space=pltpu.VMEM)
ANY = pl.BlockSpec(memory_space=pl.ANY)
SMEM = pl.BlockSpec(memory_space=pltpu.SMEM)


def call(kernel, outs, operands, specs, scratch=(), flops=0, name=None):
    return pl.pallas_call(
        kernel,
        out_shape=outs,
        in_specs=specs,
        out_specs=jax.tree.map(lambda _: VMEM, outs),
        scratch_shapes=list(scratch),
        compiler_params=pltpu.CompilerParams(vmem_limit_bytes=VMEM_LIMIT),
        cost_estimate=pl.CostEstimate(flops=flops, bytes_accessed=1 << 20, transcendentals=0),
        name=name,
    )(*operands)


def normalise(rows, gain):
    inv_rms = lax.rsqrt(jnp.mean(rows * rows, axis=-1, keepdims=True) + EPS)
    return (rows * inv_rms * gain).astype(bf16)


def head_norm(raw, gain_row, scale=1.0):
    width = raw.shape[1]
    squares = raw * raw
    high = squares.astype(bf16)
    low = (squares - high.astype(f32)).astype(bf16)
    same = (
        lax.broadcasted_iota(jnp.int32, (width, width), 0) // HEAD_DIM
        == lax.broadcasted_iota(jnp.int32, (width, width), 1) // HEAD_DIM
    ).astype(bf16)
    sums = jnp.dot(high, same, preferred_element_type=f32) + jnp.dot(
        low, same, preferred_element_type=f32
    )
    inverse = lax.rsqrt(sums * (1.0 / HEAD_DIM) + EPS)
    gains = jnp.concatenate([gain_row] * (width // HEAD_DIM), axis=1)
    normed = (raw * inverse * gains).astype(bf16)
    return normed if scale == 1.0 else normed * jnp.asarray(scale, bf16)


def column_copies(source, layer, target, sems, first, width):
    count = target.shape[1] // width
    return [
        pltpu.make_async_copy(
            source.at[layer, :, pl.ds(i * width, width)],
            target.at[:, pl.ds(i * width, width)],
            sems.at[first + i],
        )
        for i in range(count)
    ]


def write_pairs(normed, layer, width, key_gain, wk, wv, k_copies, v_copies, marks, payloads):
    tokens = normed.shape[0]
    reach = ROWS_DOWN * GRID_W
    for g, (down, up) in enumerate(payloads):
        cols = slice(g * width, (g + 1) * width)
        k_copies[g].wait()
        raw = jnp.dot(normed, wk[:, cols], preferred_element_type=f32)
        keys = head_norm(raw, key_gain[layer : layer + 1])
        down[:tokens, :width] = keys
        up[:reach, :width] = keys[:reach]
        v_copies[g].wait()
        vals = jnp.dot(normed, wv[:, cols], preferred_element_type=f32).astype(bf16)
        down[:tokens, width:] = vals
        up[:reach, width:] = vals[:reach]
        if marks is not None and g == 0:
            rows = marks[...].astype(f32) + 1.0
            rows = jnp.concatenate(
                [rows, jnp.zeros((MARK_ROWS - rows.shape[0], LANES), f32)], axis=0
            ).astype(bf16)
            down[tokens:, :LANES] = rows
            up[reach:, :LANES] = rows
            if 2 * width > LANES:
                rest = jnp.zeros((MARK_ROWS, 2 * width - LANES), bf16)
                down[tokens:, LANES:] = rest
                up[reach:, LANES:] = rest


def enter_kernel(layer, width, groups, *refs):
    h, marks, norm_gain, key_gain, w_key, w_value = refs[:6]
    normed_out = refs[6]
    payloads = [(refs[7 + 2 * g], refs[8 + 2 * g]) for g in range(groups)]
    wk, wv, sems = refs[7 + 2 * groups :]
    k_copies = column_copies(w_key, layer, wk, sems, 0, width)
    v_copies = column_copies(w_value, layer, wv, sems, groups, width)
    for k_copy, v_copy in zip(k_copies, v_copies):
        k_copy.start()
        v_copy.start()
    normed = normalise(h[...].astype(f32), norm_gain[layer : layer + 1])
    normed_out[...] = normed
    write_pairs(normed, layer, width, key_gain, wk, wv, k_copies, v_copies, marks, payloads)


def out_project(layer, parts, w_out, wo, sems, first, h, h_out, heads_all, place):
    chunk = wo.shape[1] // 4
    copies = column_copies(w_out, layer, wo, sems, first, chunk)
    for copy in copies:
        copy.start()

    def finish():
        if place is None:
            attended = parts[0][...]
        else:
            half = heads_all.shape[1] // 2
            mine = place[0] * half
            other = half - mine
            width = parts[0].shape[1]
            for g in range(len(parts) // 2):
                heads_all[:, pl.ds(pl.multiple_of(mine + g * width, width), width)] = parts[g][...]
                heads_all[:, pl.ds(pl.multiple_of(other + g * width, width), width)] = parts[
                    len(parts) // 2 + g
                ][...]
            attended = heads_all[...]
        for i, copy in enumerate(copies):
            cols = slice(i * chunk, (i + 1) * chunk)
            copy.wait()
            update = jnp.dot(attended, wo[:, cols], preferred_element_type=f32)
            h_out[:, cols] = (h[:, cols].astype(f32) + update).astype(bf16)

    return finish


def middle_kernel(layer, width, groups, part_count, placed, *refs):
    refs = list(refs)
    place = refs.pop(0) if placed else None
    parts = refs[:part_count]
    h, norm_gain, key_gain, w_out, w_key, w_value = refs[part_count : part_count + 6]
    refs = refs[part_count + 6 :]
    h_out, normed_out = refs[:2]
    payloads = [(refs[2 + 2 * g], refs[3 + 2 * g]) for g in range(groups)]
    wo, wk, wv, heads_all, sems = refs[2 + 2 * groups :]
    finish = out_project(layer - 1, parts, w_out, wo, sems, 2 * groups, h, h_out, heads_all, place)
    k_copies = column_copies(w_key, layer, wk, sems, 0, width)
    v_copies = column_copies(w_value, layer, wv, sems, groups, width)
    for k_copy, v_copy in zip(k_copies, v_copies):
        k_copy.start()
        v_copy.start()
    finish()
    normed = normalise(h_out[...].astype(f32), norm_gain[layer : layer + 1])
    normed_out[...] = normed
    write_pairs(normed, layer, width, key_gain, wk, wv, k_copies, v_copies, None, payloads)


def leave_kernel(layer, part_count, placed, *refs):
    refs = list(refs)
    place = refs.pop(0) if placed else None
    parts = refs[:part_count]
    h, w_out, h_out, wo, heads_all, sems = refs[part_count:]
    out_project(layer, parts, w_out, wo, sems, 0, h, h_out, heads_all, place)()


def query_kernel(layer, normed, query_gain, bias, w_query, q_out, table, wq, sems):
    width = wq.shape[1]
    copies = column_copies(w_query, layer, wq, sems, 0, width)
    copies[0].start()
    heads = table.shape[0]
    span = table.shape[2]
    shape = (WIN_ROWS * WIN_COLS, span)
    source = lax.broadcasted_iota(jnp.int32, shape, 0)
    lane = lax.broadcasted_iota(jnp.int32, shape, 1)
    block, lane = lane // LANES, lane % LANES
    half = WIN_COLS // 2
    low = (lane < half) | (lane >= LANES - half)
    mid = (lane >= GRID_W - half) & (lane < GRID_W + half)
    row = 2 * block + mid.astype(jnp.int32)
    col = jnp.where(mid, lane - GRID_W + half, jnp.where(lane < half, lane + half, lane - LANES + half))
    wanted = jnp.where(low | mid, row * WIN_COLS + col, -1)
    pick = (source == wanted).astype(f32)
    base = jnp.dot(
        bias[layer], pick, preferred_element_type=f32, precision=lax.Precision.HIGHEST
    )
    tile = (GRID_W, LANES)
    offset = lax.broadcasted_iota(jnp.int32, tile, 1) % GRID_W - lax.broadcasted_iota(
        jnp.int32, tile, 0
    )
    inside = (offset >= -half) & (offset < half)
    for head in range(heads):
        for p in range(span // LANES):
            cols = slice(p * LANES, (p + 1) * LANES)
            rows = jnp.broadcast_to(base[head : head + 1, cols], tile)
            rolled = pltpu.roll(rows, 0, 1, stride=1, stride_axis=0)
            table[head, :, cols] = jnp.where(inside, rolled, FAR)
    copies[0].wait()
    raw = jnp.dot(normed[...], wq[...], preferred_element_type=f32)
    q_out[...] = head_norm(raw, query_gain[layer : layer + 1], HEAD_DIM ** (-0.5))


def mark_line(payload, start, tokens):
    return [payload[start + i : start + i + 1, :LANES].astype(f32) for i in range(tokens // LANES)]


def write_mask(own, low, high, tokens, mask):
    reach = ROWS_DOWN * GRID_W
    line = mark_line(low, tokens, tokens) + mark_line(own, tokens, tokens)
    line = jnp.concatenate(line + mark_line(high, reach, tokens), axis=1)
    total = line.shape[1]
    line = jnp.broadcast_to(line, (8, total))
    own_rows = [
        jnp.broadcast_to(one, (LANES, LANES)).T for one in mark_line(own, tokens, tokens)
    ]
    own_rows = jnp.concatenate(own_rows, axis=0)
    for r in range(tokens // GRID_W):
        shifted = line if r == 0 else pltpu.roll(line, total - r * GRID_W, 1)
        mine = own_rows[r * GRID_W : (r + 1) * GRID_W]
        mine = jnp.concatenate([mine] * (WINDOW // LANES), axis=1)
        mask[r * GRID_W : (r + 1) * GRID_W] = jnp.where(mine == shifted[:1, :WINDOW], 0.0, FAR)


def attend_kernel(group, width, tokens, make_mask, *refs):
    q, table, own, low, high = refs[:5]
    if make_mask:
        out, mask = refs[5:]
        write_mask(own, low, high, tokens, mask)
    else:
        mask, out = refs[5:]
    step = min(LANES, width)
    heads = step // HEAD_DIM
    first = group * width
    ones = jnp.ones((WINDOW, step), bf16)
    for p in range(width // step):
        lanes = slice(p * step, (p + 1) * step)
        v_lanes = slice(width + p * step, width + (p + 1) * step)
        head0 = (first + p * step) // HEAD_DIM
        for r in range(tokens // GRID_W):
            mine = slice(r * GRID_W, (r + 1) * GRID_W)
            rows = q[mine, first + p * step : first + (p + 1) * step]
            pieces = [low[r * GRID_W : tokens, lanes], own[:tokens, lanes]]
            v_pieces = [low[r * GRID_W : tokens, v_lanes], own[:tokens, v_lanes]]
            if r:
                pieces.append(high[: r * GRID_W, lanes])
                v_pieces.append(high[: r * GRID_W, v_lanes])
            keys = jnp.concatenate(pieces, axis=0)
            vals = jnp.concatenate(v_pieces, axis=0)
            if heads > 1:
                lane = lax.broadcasted_iota(jnp.int32, rows.shape, 1) // HEAD_DIM
                rows = jnp.concatenate(
                    [jnp.where(lane == i, rows, jnp.zeros_like(rows)) for i in range(heads)], axis=0
                )
            scores = lax.dot_general(
                rows, keys, (((1,), (1,)), ((), ())), preferred_element_type=f32
            )
            near = mask[mine]
            scores = scores + jnp.concatenate(
                [table[head0 + i] + near for i in range(heads)], axis=0
            )
            top = jnp.max(scores, axis=1, keepdims=True)
            weights = jnp.exp(scores - top).astype(bf16)
            mixed = jnp.dot(
                weights, jnp.concatenate([vals, ones], axis=1), preferred_element_type=f32
            )
            mixed = mixed[:, :step] / mixed[:, step:]
            if heads > 1:
                lane = lax.broadcasted_iota(jnp.int32, (GRID_W, step), 1) // HEAD_DIM
                result = mixed[:GRID_W]
                for i in range(1, heads):
                    result = jnp.where(lane == i, mixed[i * GRID_W : (i + 1) * GRID_W], result)
                mixed = result
            out[mine, lanes] = mixed.astype(bf16)


def on_device(
    stream, doc_ids, norm_gain, w_query, w_key, w_value, query_gain, key_gain, offset_bias, w_output
):
    tokens, model = stream.shape
    layers, _, local = w_query.shape
    heads = local // HEAD_DIM
    every = w_output.shape[1]
    groups = 2 if local % (4 * HEAD_DIM) == 0 else 1
    width = local // groups
    reach = ROWS_DOWN * GRID_W
    ranks = lax.axis_size("sp")
    tensor = lax.axis_size("tp")
    swap = tensor == 2
    forward = [(i, i + 1) for i in range(ranks - 1)]
    backward = [(i + 1, i) for i in range(ranks - 1)]
    marks = doc_ids.reshape(tokens // LANES, LANES)
    bias = offset_bias.reshape(layers, heads, WIN_ROWS * WIN_COLS)
    place = [lax.axis_index("tp").astype(jnp.int32).reshape(1)] if swap else []
    weight = pltpu.VMEM((model, local), bf16)

    def payload_shapes(marked):
        shapes = []
        for g in range(groups):
            extra = MARK_ROWS if marked and g == 0 else 0
            shapes.append(jax.ShapeDtypeStruct((tokens + extra, 2 * width), bf16))
            shapes.append(jax.ShapeDtypeStruct((reach + extra, 2 * width), bf16))
        return shapes

    rows_shape = jax.ShapeDtypeStruct((tokens, model), bf16)
    pair_flops = 4 * tokens * model * local
    out_flops = 2 * tokens * every * model
    normed, *payloads = call(
        functools.partial(enter_kernel, 0, width, groups),
        [rows_shape] + payload_shapes(True),
        (stream, marks, norm_gain, key_gain, w_key, w_value),
        [VMEM] * 4 + [ANY] * 2,
        [weight, weight, pltpu.SemaphoreType.DMA((2 * groups,))],
        flops=pair_flops,
        name="enter",
    )
    current = stream
    mask = None
    for layer in range(layers):
        arrived = []
        for g in range(groups):
            down, up = payloads[2 * g], payloads[2 * g + 1]
            arrived.append(
                (down, lax.ppermute(down, "sp", forward), lax.ppermute(up, "sp", backward))
            )
        queries, table = call(
            functools.partial(query_kernel, layer),
            [
                jax.ShapeDtypeStruct((tokens, local), bf16),
                jax.ShapeDtypeStruct((heads, GRID_W, WINDOW), f32),
            ],
            (normed, query_gain, bias, w_query),
            [VMEM] * 3 + [ANY],
            [weight, pltpu.SemaphoreType.DMA((1,))],
            flops=pair_flops // 2,
            name="query",
        )
        attended = []
        for g in range(groups):
            make_mask = mask is None
            outs = [jax.ShapeDtypeStruct((tokens, width), bf16)]
            operands = [queries, table, *arrived[g]]
            if make_mask:
                outs.append(jax.ShapeDtypeStruct((tokens, WINDOW), f32))
            else:
                operands.append(mask)
            results = call(
                functools.partial(attend_kernel, g, width, tokens, make_mask),
                outs,
                operands,
                [VMEM] * len(operands),
                flops=4 * tokens * WINDOW * 2 * width,
                name="attend",
            )
            attended.append(results[0])
            if make_mask:
                mask = results[1]
        if swap:
            pairs = [(0, 1), (1, 0)]
            parts = attended + [lax.ppermute(part, "tp", pairs) for part in attended]
        else:
            own = attended[0] if groups == 1 else jnp.concatenate(attended, axis=1)
            parts = [lax.all_gather(own, "tp", axis=1, tiled=True)]
        whole_out = pltpu.VMEM((every, model), bf16)
        heads_all = pltpu.VMEM((tokens, every), bf16)
        if layer + 1 < layers:
            current, normed, *payloads = call(
                functools.partial(middle_kernel, layer + 1, width, groups, len(parts), swap),
                [rows_shape, rows_shape] + payload_shapes(False),
                (*place, *parts, current, norm_gain, key_gain, w_output, w_key, w_value),
                [SMEM] * len(place) + [VMEM] * (len(parts) + 3) + [ANY] * 3,
                [whole_out, weight, weight, heads_all, pltpu.SemaphoreType.DMA((2 * groups + 4,))],
                flops=pair_flops + out_flops,
                name="middle",
            )
        else:
            (current,) = call(
                functools.partial(leave_kernel, layer, len(parts), swap),
                [rows_shape],
                (*place, *parts, current, w_output),
                [SMEM] * len(place) + [VMEM] * (len(parts) + 1) + [ANY],
                [whole_out, heads_all, pltpu.SemaphoreType.DMA((4,))],
                flops=out_flops,
                name="leave",
            )
    return current


def solution(mesh):
    return jax.shard_map(
        on_device,
        mesh=mesh,
        in_specs=(
            P("sp", None),
            P("sp"),
            P(),
            P(None, None, "tp"),
            P(None, None, "tp"),
            P(None, None, "tp"),
            P(),
            P(),
            P(None, "tp", None, None),
            P(),
        ),
        out_specs=P("sp", None),
        check_vma=False,
    )
```

time: 243 us -> 80.3 us (0.33)
  the two profiles are of different devices: /device:TPU:6 before, /device:TPU:8 now
where the time goes in v1:
time: 80.3 us; the launch traced here: 79.6 us
  starting transfers between devices  26.1 us (33%)
  Pallas kernels  23.7 us (30%)
  local copies, waits for them, and re-layouts  19.3 us (24%)
  waiting for transfers between devices  10.1 us (13%)
    pallas_call x9, Pallas kernels, call(): pl.pallas_call(kernel, out_shape=outs, in_specs=specs, out_specs=jax.tree...  23.7 us
    unnamed x36, local copies, waits for them, and re-layouts  19.2 us
    ppermute x4, starting transfers between devices, on_device(): lax.ppermute(up, 'sp', backward)  11.8 us
    ppermute x4, waiting for transfers between devices, on_device(): parts = attended + [lax.ppermute(part, 'tp', pairs) for part in attended]  10 us
    ppermute x4, starting transfers between devices, on_device(): lax.ppermute(down, 'sp', forward)  9.95 us
    ppermute x4, starting transfers between devices, on_device(): parts = attended + [lax.ppermute(part, 'tp', pairs) for part in attended]  4.31 us
  transfers between devices with their start and end apart: 12, of which 4 were waited for; matrix products, arithmetic and copies ran while one was open for 0% of the time, Pallas kernels for 12%

profile of v1, /device:TPU:8, one launch (start us, length us, event | category | flops | bytes accessed | tf_op | source)
XLA Modules:
  0.0 79.6 jit_solution(14860815163779020017)
XLA Ops:
  0.0 2.2 %copy-done.3 = bf16[2,2048,512]{2,1,0:T(8,128)(2,1)S(1)} copy-done((bf16[2,2048,512]{2,1,0:T(8,128)(2,1)S(1)}, bf16[2,2048,512]{2,1,0:T(8,128)(2,1)}, u32[]{:S(2)}) %copy-start.3) | copy-done | bytes 4194328
  2.2 2.2 %copy-done.5 = bf16[2,2048,512]{2,1,0:T(8,128)(2,1)S(1)} copy-done((bf16[2,2048,512]{2,1,0:T(8,128)(2,1)S(1)}, bf16[2,2048,512]{2,1,0:T(8,128)(2,1)}, u32[]{:S(2)}) %copy-start.5) | copy-done | bytes 4194328
  4.4 1.2 %copy-done.7 = bf16[256,2048]{1,0:T(8,128)(2,1)S(1)} copy-done((bf16[256,2048]{1,0:T(8,128)(2,1)S(1)}, bf16[256,2048]{1,0:T(8,128)(2,1)}, u32[]{:S(2)}) %copy-start.7) | copy-done | bytes 1048600
  5.6 0.7 copy-done.11
  6.3 0.7 copy-done.13
  7.0 0.7 copy-done.16
  7.7 4.6 %enter.1 = (bf16[256,2048]{1,0:T(8,128)(2,1)S(1)}, bf16[272,512]{1,0:T(8,128)(2,1)S(1)}, bf16[208,512]{1,0:T(8,128)(2,1)S(1)}, bf16[256,512]{1,0:T(8,128)(2,1)S(1)}, bf16[192,512]{1,0:T(8,128)(2,1)}) custom-call(bf16[256,2048]{1,0:T(8,128)(2,1)S(1)} %copy-done.7, s32[2,128]{1,0:T(2,128)S(1)} %bitcast.4, f32[2,2048]{1,0:T(2,128)S(1)} %copy-done.11, ...), custom_call_target="tpu_custom_call" | custom-call | flops 1073741824 | bytes 1048576 | tf_op jit(solution)/shard_map/enter/pallas_call | solution.py:30
  12.3 1.9 %collective-permute-start = (bf16[272,512]{1,0:T(8,128)(2,1)S(1)}, bf16[272,512]{1,0:T(8,128)(2,1)S(1)}, u32[]{:S(2)}, u32[]{:S(2)}) collective-permute-start(bf16[272,512]{1,0:T(8,128)(2,1)S(1)} %get-tuple-element.25.refs_2_), channel_id=1, source_target_pairs={{0,2},{2,4},{4,6},{6,8},{8,10},{10,12},{12,14},{14,16},{16,18},{18... | collective-permute-start | bytes 835592 | tf_op jit(solution)/shard_map/ppermute | solution.py:333
  14.2 3.5 %collective-permute-start.2 = (bf16[256,512]{1,0:T(8,128)(2,1)S(1)}, bf16[256,512]{1,0:T(8,128)(2,1)}, u32[]{:S(2)}, u32[]{:S(2)}) collective-permute-start(bf16[256,512]{1,0:T(8,128)(2,1)S(1)} %get-tuple-element.28.refs_2_), channel_id=1, source_target_pairs={{0,2},{2,4},{4,6},{6,8},{8,10},{10,12},{12,14},{14,16},{16,18},{18... | collective-permute-start | bytes 786440 | tf_op jit(solution)/shard_map/ppermute | solution.py:333
  17.8 3.0 %collective-permute-start.1 = (bf16[208,512]{1,0:T(8,128)(2,1)S(1)}, bf16[208,512]{1,0:T(8,128)(2,1)S(1)}, u32[]{:S(2)}, u32[]{:S(2)}) collective-permute-start(bf16[208,512]{1,0:T(8,128)(2,1)S(1)} %get-tuple-element.26), channel_id=1, source_target_pairs={{2,0},{4,2},{6,4},{8,6},{10,8},{12,10},{14,12},{16,14},{18,16},{20... | collective-permute-start | bytes 638984 | tf_op jit(solution)/shard_map/ppermute | solution.py:333
  20.7 2.4 %collective-permute-start.3 = (bf16[192,512]{1,0:T(8,128)(2,1)}, bf16[192,512]{1,0:T(8,128)(2,1)}, u32[]{:S(2)}, u32[]{:S(2)}) collective-permute-start(bf16[192,512]{1,0:T(8,128)(2,1)} %get-tuple-element.29), channel_id=1, source_target_pairs={{2,0},{4,2},{6,4},{8,6},{10,8},{12,10},{14,12},{16,14},{18,16},{20... | collective-permute-start | bytes 589832 | tf_op jit(solution)/shard_map/ppermute | solution.py:333
  23.1 0.1 reshape.11.bias
  23.2 0.0 copy-start.1
  23.2 2.2 %copy-done.1 = bf16[2,2048,512]{2,1,0:T(8,128)(2,1)S(1)} copy-done((bf16[2,2048,512]{2,1,0:T(8,128)(2,1)S(1)}, bf16[2,2048,512]{2,1,0:T(8,128)(2,1)}, u32[]{:S(2)}) %copy-start.1) | copy-done | bytes 4194328
  25.4 2.0 %query.2 = (bf16[256,512]{1,0:T(8,128)(2,1)S(1)}, f32[8,64,512]{2,1,0:T(8,128)S(1)}) custom-call(bf16[256,2048]{1,0:T(8,128)(2,1)S(1)} %get-tuple-element.22.normed, f32[2,64]{1,0:T(2,128)S(1)} %copy-done.15, f32[2,8,128]{2,1,0:T(8,128)S(1)} %reshape.11.bias, bf16[2,2048,512]{2,1,0:T(8,128)(2,1)S(1)} %copy-done.1), custom_call_target="tpu_custom_call" | custom-call | flops 536870912 | bytes 1048576 | tf_op jit(solution)/shard_map/query/pallas_call | solution.py:30
  27.4 0.0 collective-permute-done.1.refs_4_
  27.4 0.0 copy-start.9
  27.4 0.7 copy-done.9
  28.1 0.0 collective-permute-done.refs_3_
  28.1 0.9 %copy-done.10 = bf16[208,512]{1,0:T(8,128)(2,1)S(1)} copy-done((bf16[208,512]{1,0:T(8,128)(2,1)S(1)}, bf16[208,512]{1,0:T(8,128)(2,1)}, u32[]{:S(2)}) %copy-start.10) | copy-done | bytes 213016
  29.0 1.2 %attend.4 = (bf16[256,256]{1,0:T(8,128)(2,1)S(1)}, f32[256,512]{1,0:T(8,128)S(1)}) custom-call(bf16[256,512]{1,0:T(8,128)(2,1)S(1)} %get-tuple-element.23.refs_0_, f32[8,64,512]{2,1,0:T(8,128)S(1)} %get-tuple-element.24.refs_1_, bf16[272,512]{1,0:T(8,128)(2,1)S(1)} %get-tuple-element.25.refs_2_, bf16[272,512]{1,0:T(8,128)(2,1)S(1)} %collective-permute-done.refs_3_, ...), custom_call_target="tpu_custom_call" | custom-call | flops 268435456 | bytes 1048576 | tf_op jit(solution)/shard_map/attend/pallas_call | solution.py:30
  30.2 1.6 %collective-permute-start.4 = (bf16[256,256]{1,0:T(8,128)(2,1)S(1)}, bf16[256,256]{1,0:T(8,128)(2,1)S(1)}, u32[]{:S(2)}, u32[]{:S(2)}) collective-permute-start(bf16[256,256]{1,0:T(8,128)(2,1)S(1)} %get-tuple-element.27.refs_1_), channel_id=1, source_target_pairs={{0,1},{1,0},{2,3},{3,2},{4,5},{5,4},{6,7},{7,6},{8,9},{9,8},{10,11... | collective-permute-start | bytes 393224 | tf_op jit(solution)/shard_map/ppermute | solution.py:369
  31.8 0.0 collective-permute-done.3.refs_4_
  31.8 0.0 collective-permute-done.2.refs_3_
  31.8 2.1 %attend.5.refs_2_ = bf16[256,256]{1,0:T(8,128)(2,1)S(1)} custom-call(bf16[256,512]{1,0:T(8,128)(2,1)S(1)} %get-tuple-element.23.refs_0_, f32[8,64,512]{2,1,0:T(8,128)S(1)} %get-tuple-element.24.refs_1_, bf16[256,512]{1,0:T(8,128)(2,1)S(1)} %get-tuple-element.28.refs_2_, bf16[256,512]{1,0:T(8,128)(2,1)} %collective-permute-done.2.refs_3_, ...), custom_call_target="tpu_custom_call" | custom-call | flops 268435456 | bytes 1048576 | tf_op jit(solution)/shard_map/attend/pallas_call | solution.py:30
  34.0 0.6 collective-permute-start.5
  34.5 1.2 %collective-permute-done.4.refs_3_ = bf16[256,256]{1,0:T(8,128)(2,1)S(1)} collective-permute-done((bf16[256,256]{1,0:T(8,128)(2,1)S(1)}, bf16[256,256]{1,0:T(8,128)(2,1)S(1)}, u32[]{:S(2)}, u32[]{:S(2)}) %collective-permute-start.4) | collective-permute-done | bytes 131104 | tf_op jit(solution)/shard_map/ppermute | solution.py:369
  35.7 3.4 %collective-permute-done.5.refs_4_ = bf16[256,256]{1,0:T(8,128)(2,1)S(1)} collective-permute-done((bf16[256,256]{1,0:T(8,128)(2,1)S(1)}, bf16[256,256]{1,0:T(8,128)(2,1)S(1)}, u32[]{:S(2)}, u32[]{:S(2)}) %collective-permute-start.5) | collective-permute-done | bytes 131104 | tf_op jit(solution)/shard_map/ppermute | solution.py:369
  39.2 0.0 copy-start
  39.2 3.4 %copy-done = bf16[2,1024,2048]{2,1,0:T(8,128)(2,1)S(1)} copy-done((bf16[2,1024,2048]{2,1,0:T(8,128)(2,1)S(1)}, bf16[2,1024,2048]{2,1,0:T(8,128)(2,1)}, u32[]{:S(2)}) %copy-start) | copy-done | bytes 8388632
  42.6 2.2 %copy-done.4 = bf16[2,2048,512]{2,1,0:T(8,128)(2,1)S(1)} copy-done((bf16[2,2048,512]{2,1,0:T(8,128)(2,1)S(1)}, bf16[2,2048,512]{2,1,0:T(8,128)(2,1)}, u32[]{:S(2)}) %copy-start.4) | copy-done | bytes 4194328
  44.7 2.2 %copy-done.6 = bf16[2,2048,512]{2,1,0:T(8,128)(2,1)S(1)} copy-done((bf16[2,2048,512]{2,1,0:T(8,128)(2,1)S(1)}, bf16[2,2048,512]{2,1,0:T(8,128)(2,1)}, u32[]{:S(2)}) %copy-start.6) | copy-done | bytes 4194328
  46.9 6.4 %middle.1 = (bf16[256,2048]{1,0:T(8,128)(2,1)S(1)}, bf16[256,2048]{1,0:T(8,128)(2,1)S(1)}, bf16[256,512]{1,0:T(8,128)(2,1)S(1)}, bf16[192,512]{1,0:T(8,128)(2,1)...) custom-call(s32[1]{0:T(128)} %bitcast.refs_0_, bf16[256,256]{1,0:T(8,128)(2,1)S(1)} %get-tuple-element.27.refs_1_, ...), custom_call_target="tpu_custom_call" | custom-call | flops 2147483648 | bytes 1048576 | tf_op jit(solution)/shard_map/middle/pallas_call | solution.py:30
  53.3 1.9 %collective-permute-start.6 = (bf16[256,512]{1,0:T(8,128)(2,1)S(1)}, bf16[256,512]{1,0:T(8,128)(2,1)S(1)}, u32[]{:S(2)}, u32[]{:S(2)}) collective-permute-start(bf16[256,512]{1,0:T(8,128)(2,1)S(1)} %get-tuple-element.34.refs_2_), channel_id=1, source_target_pairs={{0,2},{2,4},{4,6},{6,8},{8,10},{10,12},{12,14},{14,16},{16,18},{18... | collective-permute-start | bytes 786440 | tf_op jit(solution)/shard_map/ppermute | solution.py:333
  55.3 2.6 %collective-permute-start.8 = (bf16[256,512]{1,0:T(8,128)(2,1)S(1)}, bf16[256,512]{1,0:T(8,128)(2,1)S(1)}, u32[]{:S(2)}, u32[]{:S(2)}) collective-permute-start(bf16[256,512]{1,0:T(8,128)(2,1)S(1)} %get-tuple-element.36.refs_2_), channel_id=1, source_target_pairs={{0,2},{2,4},{4,6},{6,8},{8,10},{10,12},{12,14},{14,16},{16,18},{18... | collective-permute-start | bytes 786440 | tf_op jit(solution)/shard_map/ppermute | solution.py:333
  57.9 3.9 %collective-permute-start.7 = (bf16[192,512]{1,0:T(8,128)(2,1)S(1)}, bf16[192,512]{1,0:T(8,128)(2,1)S(1)}, u32[]{:S(2)}, u32[]{:S(2)}) collective-permute-start(bf16[192,512]{1,0:T(8,128)(2,1)S(1)} %get-tuple-element.35), channel_id=1, source_target_pairs={{2,0},{4,2},{6,4},{8,6},{10,8},{12,10},{14,12},{16,14},{18,16},{20... | collective-permute-start | bytes 589832 | tf_op jit(solution)/shard_map/ppermute | solution.py:333
  61.8 2.6 %collective-permute-start.9 = (bf16[192,512]{1,0:T(8,128)(2,1)S(1)}, bf16[192,512]{1,0:T(8,128)(2,1)S(1)}, u32[]{:S(2)}, u32[]{:S(2)}) collective-permute-start(bf16[192,512]{1,0:T(8,128)(2,1)S(1)} %get-tuple-element.37), channel_id=1, source_target_pairs={{2,0},{4,2},{6,4},{8,6},{10,8},{12,10},{14,12},{16,14},{18,16},{20... | collective-permute-start | bytes 589832 | tf_op jit(solution)/shard_map/ppermute | solution.py:333
  64.4 2.0 %query.3 = (bf16[256,512]{1,0:T(8,128)(2,1)S(1)}, f32[8,64,512]{2,1,0:T(8,128)S(1)}) custom-call(bf16[256,2048]{1,0:T(8,128)(2,1)S(1)} %get-tuple-element.31.normed, f32[2,64]{1,0:T(2,128)S(1)} %copy-done.15, f32[2,8,128]{2,1,0:T(8,128)S(1)} %reshape.11.bias, bf16[2,2048,512]{2,1,0:T(8,128)(2,1)S(1)} %copy-done.2), custom_call_target="tpu_custom_call" | custom-call | flops 536870912 | bytes 1048576 | tf_op jit(solution)/shard_map/query/pallas_call | solution.py:30
  66.3 0.0 collective-permute-done.7.refs_4_
  66.4 1.0 %attend.6.refs_1_ = bf16[256,256]{1,0:T(8,128)(2,1)S(1)} custom-call(bf16[256,512]{1,0:T(8,128)(2,1)S(1)} %get-tuple-element.32.refs_0_, f32[8,64,512]{2,1,0:T(8,128)S(1)} %get-tuple-element.33.refs_1_, bf16[256,512]{1,0:T(8,128)(2,1)S(1)} %get-tuple-element.34.refs_2_, bf16[256,512]{1,0:T(8,128)(2,1)S(1)} %collective-permute-done.6.refs_3_, ...), custom_call_target="tpu_custom_call" | custom-call | flops 268435456 | bytes 1048576 | tf_op jit(solution)/shard_map/attend/pallas_call | solution.py:30
  67.4 1.0 %collective-permute-start.10 = (bf16[256,256]{1,0:T(8,128)(2,1)S(1)}, bf16[256,256]{1,0:T(8,128)(2,1)S(1)}, u32[]{:S(2)}, u32[]{:S(2)}) collective-permute-start(bf16[256,256]{1,0:T(8,128)(2,1)S(1)} %attend.6.refs_1_), channel_id=1, source_target_pairs={{0,1},{1,0},{2,3},{3,2},{4,5},{5,4},{6,7},{7,6},{8,9},{9,8},{10,11... | collective-permute-start | bytes 393224 | tf_op jit(solution)/shard_map/ppermute | solution.py:369
  68.4 0.0 collective-permute-done.9.refs_4_
  68.4 0.0 collective-permute-done.8.refs_3_
  68.4 1.0 %attend.7.refs_2_ = bf16[256,256]{1,0:T(8,128)(2,1)S(1)} custom-call(bf16[256,512]{1,0:T(8,128)(2,1)S(1)} %get-tuple-element.32.refs_0_, f32[8,64,512]{2,1,0:T(8,128)S(1)} %get-tuple-element.33.refs_1_, bf16[256,512]{1,0:T(8,128)(2,1)S(1)} %get-tuple-element.36.refs_2_, bf16[256,512]{1,0:T(8,128)(2,1)S(1)} %collective-permute-done.8.refs_3_, ...), custom_call_target="tpu_custom_call" | custom-call | flops 268435456 | bytes 1048576 | tf_op jit(solution)/shard_map/attend/pallas_call | solution.py:30
  69.4 1.2 %collective-permute-start.11 = (bf16[256,256]{1,0:T(8,128)(2,1)S(1)}, bf16[256,256]{1,0:T(8,128)(2,1)S(1)}, u32[]{:S(2)}, u32[]{:S(2)}) collective-permute-start(bf16[256,256]{1,0:T(8,128)(2,1)S(1)} %attend.7.refs_2_), channel_id=1, source_target_pairs={{0,1},{1,0},{2,3},{3,2},{4,5},{5,4},{6,7},{7,6},{8,9},{9,8},{10,11... | collective-permute-start | bytes 393224 | tf_op jit(solution)/shard_map/ppermute | solution.py:369
  70.6 3.3 %collective-permute-done.10.refs_3_ = bf16[256,256]{1,0:T(8,128)(2,1)S(1)} collective-permute-done((bf16[256,256]{1,0:T(8,128)(2,1)S(1)}, bf16[256,256]{1,0:T(8,128)(2,1)S(1)}, u32[]{:S(2)}, u32[]{:S(2)}) %collective-permute-start.10) | collective-permute-done | bytes 131104 | tf_op jit(solution)/shard_map/ppermute | solution.py:369
  73.8 2.2 %collective-permute-done.11.refs_4_ = bf16[256,256]{1,0:T(8,128)(2,1)S(1)} collective-permute-done((bf16[256,256]{1,0:T(8,128)(2,1)S(1)}, bf16[256,256]{1,0:T(8,128)(2,1)S(1)}, u32[]{:S(2)}, u32[]{:S(2)}) %collective-permute-start.11) | collective-permute-done | bytes 131104 | tf_op jit(solution)/shard_map/ppermute | solution.py:369
  76.0 3.4 %leave.1 = bf16[256,2048]{1,0:T(8,128)(2,1)} custom-call(s32[1]{0:T(128)} %bitcast.refs_0_, bf16[256,256]{1,0:T(8,128)(2,1)S(1)} %attend.6.refs_1_, bf16[256,256]{1,0:T(8,128)(2,1)S(1)} %attend.7.refs_2_, bf16[256,256]{1,0:T(8,128)(2,1)S(1)} %collective-permute-done.10.refs_3_, bf16[256,256]{1,0:T(8,128)(2,1)S(1)} %collective-permute-done.11.refs_4_, ...), custom_call_target="tpu_custom_call" | custom-call | flops 1073741824 | bytes 1048576 | tf_op jit(solution)/shard_map/leave/pallas_call | solution.py:30
  (22 shorter events, 0.0 us)
Async XLA Ops:
  0.0 2.2 %copy-start.3 = (bf16[2,2048,512]{2,1,0:T(8,128)(2,1)S(1)}, bf16[2,2048,512]{2,1,0:T(8,128)(2,1)}, u32[]{:S(2)}) copy-start(bf16[2,2048,512]{2,1,0:T(8,128)(2,1)} %refs_9_.1) | copy-start | bytes 12582916
  2.2 2.2 %copy-start.5 = (bf16[2,2048,512]{2,1,0:T(8,128)(2,1)S(1)}, bf16[2,2048,512]{2,1,0:T(8,128)(2,1)}, u32[]{:S(2)}) copy-start(bf16[2,2048,512]{2,1,0:T(8,128)(2,1)} %refs_10_.1) | copy-start | bytes 12582916
  4.4 1.2 %copy-start.7 = (bf16[256,2048]{1,0:T(8,128)(2,1)S(1)}, bf16[256,2048]{1,0:T(8,128)(2,1)}, u32[]{:S(2)}) copy-start(bf16[256,2048]{1,0:T(8,128)(2,1)} %refs_5_.3) | copy-start | bytes 3145732
  5.6 0.7 copy-start.11
  6.3 0.7 copy-start.13
  7.0 0.7 copy-start.16
  7.7 15.5 %copy-start.17 = (f32[2,8,8,16]{3,2,1,0:T(8,128)S(1)}, f32[2,8,8,16]{3,2,1,0:T(8,128)}, u32[]{:S(2)}) copy-start(f32[2,8,8,16]{3,2,1,0:T(8,128)} %param.18) | copy-start | bytes 24580
  7.7 15.5 %copy-start.15 = (f32[2,64]{1,0:T(2,128)S(1)}, f32[2,64]{1,0:T(2,128)}, u32[]{:S(2)}) copy-start(f32[2,64]{1,0:T(2,128)} %query_gain.3) | copy-start | bytes 1540
  12.3 15.8 %collective-permute-start = (bf16[272,512]{1,0:T(8,128)(2,1)S(1)}, bf16[272,512]{1,0:T(8,128)(2,1)S(1)}, u32[]{:S(2)}, u32[]{:S(2)}) collective-permute-start(bf16[272,512]{1,0:T(8,128)(2,1)S(1)} %get-tuple-element.25.refs_2_), channel_id=1, source_target_pairs={{0,2},{2,4},{4,6},{6,8},{8,10},{10,12},{12,14},{14,16},{16,18},{18... | collective-permute-start | bytes 835592 | tf_op jit(solution)/shard_map/ppermute | solution.py:333
  14.2 17.6 %collective-permute-start.2 = (bf16[256,512]{1,0:T(8,128)(2,1)S(1)}, bf16[256,512]{1,0:T(8,128)(2,1)}, u32[]{:S(2)}, u32[]{:S(2)}) collective-permute-start(bf16[256,512]{1,0:T(8,128)(2,1)S(1)} %get-tuple-element.28.refs_2_), channel_id=1, source_target_pairs={{0,2},{2,4},{4,6},{6,8},{8,10},{10,12},{12,14},{14,16},{16,18},{18... | collective-permute-start | bytes 786440 | tf_op jit(solution)/shard_map/ppermute | solution.py:333
  17.8 9.7 %collective-permute-start.1 = (bf16[208,512]{1,0:T(8,128)(2,1)S(1)}, bf16[208,512]{1,0:T(8,128)(2,1)S(1)}, u32[]{:S(2)}, u32[]{:S(2)}) collective-permute-start(bf16[208,512]{1,0:T(8,128)(2,1)S(1)} %get-tuple-element.26), channel_id=1, source_target_pairs={{2,0},{4,2},{6,4},{8,6},{10,8},{12,10},{14,12},{16,14},{18,16},{20... | collective-permute-start | bytes 638984 | tf_op jit(solution)/shard_map/ppermute | solution.py:333
  20.7 11.1 %collective-permute-start.3 = (bf16[192,512]{1,0:T(8,128)(2,1)}, bf16[192,512]{1,0:T(8,128)(2,1)}, u32[]{:S(2)}, u32[]{:S(2)}) collective-permute-start(bf16[192,512]{1,0:T(8,128)(2,1)} %get-tuple-element.29), channel_id=1, source_target_pairs={{2,0},{4,2},{6,4},{8,6},{10,8},{12,10},{14,12},{16,14},{18,16},{20... | collective-permute-start | bytes 589832 | tf_op jit(solution)/shard_map/ppermute | solution.py:333
  23.2 2.2 %copy-start.1 = (bf16[2,2048,512]{2,1,0:T(8,128)(2,1)S(1)}, bf16[2,2048,512]{2,1,0:T(8,128)(2,1)}, u32[]{:S(2)}) copy-start(bf16[2,2048,512]{2,1,0:T(8,128)(2,1)} %w_query.3) | copy-start | bytes 12582916
  25.4 13.7 %copy-start.8 = (bf16[256,2048]{1,0:T(8,128)(2,1)S(1)}, bf16[256,2048]{1,0:T(8,128)(2,1)}, u32[]{:S(2)}) copy-start(bf16[256,2048]{1,0:T(8,128)(2,1)} %refs_5_.3) | copy-start | bytes 3145732
  25.4 13.7 %copy-start.12 = (f32[2,2048]{1,0:T(2,128)S(1)}, f32[2,2048]{1,0:T(2,128)}, u32[]{:S(2)}) copy-start(f32[2,2048]{1,0:T(2,128)} %refs_6_.2) | copy-start | bytes 49156
  25.4 13.7 %copy-start.14 = (f32[2,64]{1,0:T(2,128)S(1)}, f32[2,64]{1,0:T(2,128)}, u32[]{:S(2)}) copy-start(f32[2,64]{1,0:T(2,128)} %refs_7_.1) | copy-start | bytes 1540
  27.4 0.7 copy-start.9
  28.1 0.9 %copy-start.10 = (bf16[208,512]{1,0:T(8,128)(2,1)S(1)}, bf16[208,512]{1,0:T(8,128)(2,1)}, u32[]{:S(2)}) copy-start(bf16[208,512]{1,0:T(8,128)(2,1)} %copy-done.9) | copy-start | bytes 638980
  30.2 5.5 %collective-permute-start.4 = (bf16[256,256]{1,0:T(8,128)(2,1)S(1)}, bf16[256,256]{1,0:T(8,128)(2,1)S(1)}, u32[]{:S(2)}, u32[]{:S(2)}) collective-permute-start(bf16[256,256]{1,0:T(8,128)(2,1)S(1)} %get-tuple-element.27.refs_1_), channel_id=1, source_target_pairs={{0,1},{1,0},{2,3},{3,2},{4,5},{5,4},{6,7},{7,6},{8,9},{9,8},{10,11... | collective-permute-start | bytes 393224 | tf_op jit(solution)/shard_map/ppermute | solution.py:369
  34.0 5.2 %collective-permute-start.5 = (bf16[256,256]{1,0:T(8,128)(2,1)S(1)}, bf16[256,256]{1,0:T(8,128)(2,1)S(1)}, u32[]{:S(2)}, u32[]{:S(2)}) collective-permute-start(bf16[256,256]{1,0:T(8,128)(2,1)S(1)} %attend.5.refs_2_), channel_id=1, source_target_pairs={{0,1},{1,0},{2,3},{3,2},{4,5},{5,4},{6,7},{7,6},{8,9},{9,8},{10,11... | collective-permute-start | bytes 393224 | tf_op jit(solution)/shard_map/ppermute | solution.py:369
  39.2 3.4 %copy-start = (bf16[2,1024,2048]{2,1,0:T(8,128)(2,1)S(1)}, bf16[2,1024,2048]{2,1,0:T(8,128)(2,1)}, u32[]{:S(2)}) copy-start(bf16[2,1024,2048]{2,1,0:T(8,128)(2,1)} %refs_6_.3) | copy-start | bytes 25165828
  42.5 2.2 %copy-start.4 = (bf16[2,2048,512]{2,1,0:T(8,128)(2,1)S(1)}, bf16[2,2048,512]{2,1,0:T(8,128)(2,1)}, u32[]{:S(2)}) copy-start(bf16[2,2048,512]{2,1,0:T(8,128)(2,1)} %refs_9_.1) | copy-start | bytes 12582916
  44.7 2.2 %copy-start.6 = (bf16[2,2048,512]{2,1,0:T(8,128)(2,1)S(1)}, bf16[2,2048,512]{2,1,0:T(8,128)(2,1)}, u32[]{:S(2)}) copy-start(bf16[2,2048,512]{2,1,0:T(8,128)(2,1)} %refs_10_.1) | copy-start | bytes 12582916
  46.9 17.4 %copy-start.2 = (bf16[2,2048,512]{2,1,0:T(8,128)(2,1)S(1)}, bf16[2,2048,512]{2,1,0:T(8,128)(2,1)}, u32[]{:S(2)}) copy-start(bf16[2,2048,512]{2,1,0:T(8,128)(2,1)} %w_query.3) | copy-start | bytes 12582916
  53.3 13.0 %collective-permute-start.6 = (bf16[256,512]{1,0:T(8,128)(2,1)S(1)}, bf16[256,512]{1,0:T(8,128)(2,1)S(1)}, u32[]{:S(2)}, u32[]{:S(2)}) collective-permute-start(bf16[256,512]{1,0:T(8,128)(2,1)S(1)} %get-tuple-element.34.refs_2_), channel_id=1, source_target_pairs={{0,2},{2,4},{4,6},{6,8},{8,10},{10,12},{12,14},{14,16},{16,18},{18... | collective-permute-start | bytes 786440 | tf_op jit(solution)/shard_map/ppermute | solution.py:333
  55.3 13.1 %collective-permute-start.8 = (bf16[256,512]{1,0:T(8,128)(2,1)S(1)}, bf16[256,512]{1,0:T(8,128)(2,1)S(1)}, u32[]{:S(2)}, u32[]{:S(2)}) collective-permute-start(bf16[256,512]{1,0:T(8,128)(2,1)S(1)} %get-tuple-element.36.refs_2_), channel_id=1, source_target_pairs={{0,2},{2,4},{4,6},{6,8},{8,10},{10,12},{12,14},{14,16},{16,18},{18... | collective-permute-start | bytes 786440 | tf_op jit(solution)/shard_map/ppermute | solution.py:333
  57.9 8.5 %collective-permute-start.7 = (bf16[192,512]{1,0:T(8,128)(2,1)S(1)}, bf16[192,512]{1,0:T(8,128)(2,1)S(1)}, u32[]{:S(2)}, u32[]{:S(2)}) collective-permute-start(bf16[192,512]{1,0:T(8,128)(2,1)S(1)} %get-tuple-element.35), channel_id=1, source_target_pairs={{2,0},{4,2},{6,4},{8,6},{10,8},{12,10},{14,12},{16,14},{18,16},{20... | collective-permute-start | bytes 589832 | tf_op jit(solution)/shard_map/ppermute | solution.py:333
  61.8 6.6 %collective-permute-start.9 = (bf16[192,512]{1,0:T(8,128)(2,1)S(1)}, bf16[192,512]{1,0:T(8,128)(2,1)S(1)}, u32[]{:S(2)}, u32[]{:S(2)}) collective-permute-start(bf16[192,512]{1,0:T(8,128)(2,1)S(1)} %get-tuple-element.37), channel_id=1, source_target_pairs={{2,0},{4,2},{6,4},{8,6},{10,8},{12,10},{14,12},{16,14},{18,16},{20... | collective-permute-start | bytes 589832 | tf_op jit(solution)/shard_map/ppermute | solution.py:333
  67.4 6.4 %collective-permute-start.10 = (bf16[256,256]{1,0:T(8,128)(2,1)S(1)}, bf16[256,256]{1,0:T(8,128)(2,1)S(1)}, u32[]{:S(2)}, u32[]{:S(2)}) collective-permute-start(bf16[256,256]{1,0:T(8,128)(2,1)S(1)} %attend.6.refs_1_), channel_id=1, source_target_pairs={{0,1},{1,0},{2,3},{3,2},{4,5},{5,4},{6,7},{7,6},{8,9},{9,8},{10,11... | collective-permute-start | bytes 393224 | tf_op jit(solution)/shard_map/ppermute | solution.py:369
  69.4 6.6 %collective-permute-start.11 = (bf16[256,256]{1,0:T(8,128)(2,1)S(1)}, bf16[256,256]{1,0:T(8,128)(2,1)S(1)}, u32[]{:S(2)}, u32[]{:S(2)}) collective-permute-start(bf16[256,256]{1,0:T(8,128)(2,1)S(1)} %attend.7.refs_2_), channel_id=1, source_target_pairs={{0,1},{1,0},{2,3},{3,2},{4,5},{5,4},{6,7},{7,6},{8,9},{9,8},{10,11... | collective-permute-start | bytes 393224 | tf_op jit(solution)/shard_map/ppermute | solution.py:369
